TPU v7x, 32 devices: a whole 2x2x4 slice. The times are simulated.
32 devices in a mesh: kv: 8 (over z, y), tp: 4 (over x, core).
Axes of the slice: x: 2, y: 2, z: 4, core: 2. Of those that a mesh axis runs over, the one named last changes fastest.
Arguments:
- hidden_rows: bfloat16 [8192, 4096], P(('kv', 'tp')), may hold values from -6 to 6
- queries: bfloat16 [8192, 4096], P('kv', 'tp'), may hold values from -6 to 6
- key_rows: bfloat16 [8192, 1024], P('kv', 'tp'), may hold values from -6 to 6
- value_rows: bfloat16 [8192, 1024], P('kv', 'tp'), may hold values from -6 to 6
- branch_gates: float32 [2, 32, 8192], P(None, 'tp', 'kv'), may hold values from 0.05 to 0.95
- log_sums: float32 [2, 32, 8192], P(None, 'tp', 'kv'), may hold values from 1 to 7
- chosen: int32 [8, 64, 16], P('tp', 'kv'), may hold values from 0 to 255, as said below
- out_grad: bfloat16 [8192, 4096], P('kv', 'tp'), may hold values from -6 to 6
Outputs:
- grad_queries: bfloat16 [8192, 4096], P('kv', 'tp')
- grad_keys: bfloat16 [8192, 1024], P('kv', 'tp')
- grad_values: bfloat16 [8192, 1024], P('kv', 'tp')
- grad_weight: float32 [4096, 4096], P('kv', 'tp')
Inputs may be any that keep to these rules, and one draw needn't show every extreme that they name: `chosen`: each list names distinct key blocks, among them the blocks that cover the query block's own rows; blocks past a query's position may be named and carry no weight for it. For one key head, the lists of the query blocks of one index of kv name at most 16 key blocks (counted with repetition) that lie at any one other index of kv.
All inputs are finite; a program needn't handle non-finite values.
Results may differ from a plain program's by a relative error of at most 0.011.
Values may be sent and summed in bfloat16 or wider, within the bound.
A program may use at most 128 MiB of HBM per device.

v0:
```python
import jax
import jax.numpy as jnp
from jax import lax
from jax.sharding import PartitionSpec as P

HEADS = 32
KV_HEADS = 8
HEAD_DIM = 128
QUERY_BLOCK = 128
KEY_BLOCK = 32
POOL_BLOCK = 32
CHOSEN = 16
CAP = 16


def attend_back(query_rows, key_set, value_set, cotangent, log_sum, visible, score_scale):
    scores = (
        jnp.einsum("bgrd,bmd->bgrm", query_rows, key_set, preferred_element_type=jnp.float32)
        * score_scale
    )
    weights = jnp.where(visible[:, None], jnp.exp(scores - log_sum[..., None]), 0.0)
    weights_low = weights.astype(jnp.bfloat16)
    branch_out = jnp.einsum(
        "bgrm,bmd->bgrd", weights_low, value_set, preferred_element_type=jnp.float32
    )
    row_delta = jnp.sum(cotangent.astype(jnp.float32) * branch_out, axis=-1)
    grad_prob = jnp.einsum(
        "bgrd,bmd->bgrm", cotangent, value_set, preferred_element_type=jnp.float32
    )
    dscore = (weights * (grad_prob - row_delta[..., None])).astype(jnp.bfloat16)
    dquery = (
        jnp.einsum("bgrm,bmd->bgrd", dscore, key_set, preferred_element_type=jnp.float32)
        * score_scale
    )
    grad_key = (
        jnp.einsum("bgrm,bgrd->bmd", dscore, query_rows, preferred_element_type=jnp.float32)
        * score_scale
    )
    grad_value = jnp.einsum(
        "bgrm,bgrd->bmd", weights_low, cotangent, preferred_element_type=jnp.float32
    )
    return (dquery, grad_key, grad_value)


def body(hidden_rows, queries, key_rows, value_rows, branch_gates, log_sums, chosen, out_grad):
    kv_count = lax.axis_size("kv")
    kv_index = lax.axis_index("kv")
    tokens = queries.shape[0]
    kv_local = key_rows.shape[1] // HEAD_DIM
    group_size = HEADS // KV_HEADS
    score_scale = HEAD_DIM ** (-0.5)
    seq_len = tokens * kv_count
    per_device = tokens // QUERY_BLOCK
    blocks_here = tokens // KEY_BLOCK
    request_count = per_device * CHOSEN
    positions = kv_index * tokens + jnp.arange(tokens, dtype=jnp.int32)
    key_heads = key_rows.reshape(tokens, kv_local, HEAD_DIM).transpose(1, 0, 2)
    value_heads = value_rows.reshape(tokens, kv_local, HEAD_DIM).transpose(1, 0, 2)
    query_heads = queries.reshape(tokens, kv_local, group_size, HEAD_DIM).transpose(1, 2, 0, 3)
    grad_heads = (
        out_grad.reshape(tokens, kv_local, group_size, HEAD_DIM)
        .transpose(1, 2, 0, 3)
        .astype(jnp.float32)
    )
    gate_heads = branch_gates.reshape(2, kv_local, group_size, tokens)
    sum_heads = log_sums.reshape(2, kv_local, group_size, tokens)
    cot_pool = (gate_heads[0][..., None] * grad_heads).astype(jnp.bfloat16)
    cot_chosen = (gate_heads[1][..., None] * grad_heads).astype(jnp.bfloat16)
    pooled_keys = jnp.mean(
        key_heads.astype(jnp.float32).reshape(kv_local, tokens // POOL_BLOCK, POOL_BLOCK, HEAD_DIM),
        axis=2,
    ).astype(jnp.bfloat16)
    pooled_values = jnp.mean(
        value_heads.astype(jnp.float32).reshape(
            kv_local, tokens // POOL_BLOCK, POOL_BLOCK, HEAD_DIM
        ),
        axis=2,
    ).astype(jnp.bfloat16)
    every_pooled_keys, every_pooled_values = (
        lax.all_gather(pooled_keys, "kv", axis=1, tiled=True),
        lax.all_gather(pooled_values, "kv", axis=1, tiled=True),
    )
    pool_end = jnp.arange(seq_len // POOL_BLOCK, dtype=jnp.int32) * POOL_BLOCK + POOL_BLOCK - 1
    pool_visible = (pool_end[None, :] <= positions[:, None])[None]
    pool_dquery, pool_dkeys, pool_dvalues = attend_back(
        query_heads,
        every_pooled_keys,
        every_pooled_values,
        cot_pool,
        sum_heads[0],
        pool_visible,
        score_scale,
    )
    pool_dkeys_here, pool_dvalues_here = (
        lax.psum_scatter(
            pool_dkeys.astype(jnp.bfloat16), "kv", scatter_dimension=1, tiled=True
        ).astype(jnp.float32),
        lax.psum_scatter(
            pool_dvalues.astype(jnp.bfloat16), "kv", scatter_dimension=1, tiled=True
        ).astype(jnp.float32),
    )
    head_index = jnp.arange(kv_local, dtype=jnp.int32)[:, None]
    block_lists = chosen.reshape(kv_local, request_count)
    key_positions = (
        block_lists[..., None] * KEY_BLOCK + jnp.arange(KEY_BLOCK, dtype=jnp.int32)
    ).reshape(kv_local, per_device, CHOSEN * KEY_BLOCK)
    query_positions = positions.reshape(per_device, QUERY_BLOCK)
    chosen_visible = (key_positions[:, :, None, :] <= query_positions[None, :, :, None]).reshape(
        kv_local * per_device, QUERY_BLOCK, CHOSEN * KEY_BLOCK
    )

    def regroup(heads):
        split_rows = heads.reshape(kv_local, group_size, per_device, QUERY_BLOCK, heads.shape[-1])
        return split_rows.transpose(0, 2, 1, 3, 4).reshape(
            kv_local * per_device, group_size, QUERY_BLOCK, heads.shape[-1]
        )

    chosen_sums = regroup(sum_heads[1][..., None])[..., 0]
    owners = block_lists // blocks_here
    local_block = block_lists % blocks_here
    remote = owners != kv_index
    owner_hits = (owners[..., None] == jnp.arange(kv_count, dtype=jnp.int32)).astype(jnp.int32)
    rank_in = jnp.sum(owner_hits * (jnp.cumsum(owner_hits, axis=1) - 1), axis=-1)
    slot_count = kv_count * CAP
    slot_index = jnp.where(remote, owners * CAP + rank_in, slot_count)
    wanted = (
        jnp.zeros((kv_local, slot_count), jnp.int32)
        .at[head_index, slot_index]
        .set(local_block, mode="drop")
    )
    asked_for = lax.all_to_all(wanted, "kv", split_axis=1, concat_axis=1, tiled=True)
    key_blocks = key_heads.reshape(kv_local, blocks_here, KEY_BLOCK, HEAD_DIM)
    value_blocks = value_heads.reshape(kv_local, blocks_here, KEY_BLOCK, HEAD_DIM)
    sent_keys, sent_values = (
        lax.all_to_all(
            key_blocks[head_index, asked_for], "kv", split_axis=1, concat_axis=1, tiled=True
        ),
        lax.all_to_all(
            value_blocks[head_index, asked_for], "kv", split_axis=1, concat_axis=1, tiled=True
        ),
    )
    table_index = jnp.where(remote, blocks_here + slot_index, local_block)
    key_table = jnp.concatenate([key_blocks, sent_keys], axis=1)
    value_table = jnp.concatenate([value_blocks, sent_values], axis=1)
    dquery, grad_key, grad_value = attend_back(
        regroup(query_heads),
        key_table[head_index, table_index].reshape(
            kv_local * per_device, CHOSEN * KEY_BLOCK, HEAD_DIM
        ),
        value_table[head_index, table_index].reshape(
            kv_local * per_device, CHOSEN * KEY_BLOCK, HEAD_DIM
        ),
        regroup(cot_chosen),
        chosen_sums,
        chosen_visible,
        score_scale,
    )
    dquery = (
        dquery.reshape(kv_local, per_device, group_size, QUERY_BLOCK, HEAD_DIM)
        .transpose(0, 2, 1, 3, 4)
        .reshape(kv_local, group_size, tokens, HEAD_DIM)
    )
    pick_dquery, grad_key, grad_value = (
        dquery,
        grad_key.reshape(kv_local, request_count, KEY_BLOCK, HEAD_DIM),
        grad_value.reshape(kv_local, request_count, KEY_BLOCK, HEAD_DIM),
    )
    own_index = jnp.where(remote, blocks_here, local_block)
    pick_dkeys = (
        jnp.zeros((kv_local, blocks_here, KEY_BLOCK, HEAD_DIM), jnp.float32)
        .at[head_index, own_index]
        .add(grad_key, mode="drop")
    )
    pick_dvalues = (
        jnp.zeros((kv_local, blocks_here, KEY_BLOCK, HEAD_DIM), jnp.float32)
        .at[head_index, own_index]
        .add(grad_value, mode="drop")
    )
    back_keys = (
        jnp.zeros((kv_local, slot_count, KEY_BLOCK, HEAD_DIM), jnp.float32)
        .at[head_index, slot_index]
        .set(grad_key, mode="drop")
    )
    back_values = (
        jnp.zeros((kv_local, slot_count, KEY_BLOCK, HEAD_DIM), jnp.float32)
        .at[head_index, slot_index]
        .set(grad_value, mode="drop")
    )
    got_keys, got_values = (
        lax.all_to_all(back_keys, "kv", split_axis=1, concat_axis=1, tiled=True),
        lax.all_to_all(back_values, "kv", split_axis=1, concat_axis=1, tiled=True),
    )
    owner_onehot = (
        asked_for[:, None, :] == jnp.arange(blocks_here, dtype=jnp.int32)[None, :, None]
    ).astype(jnp.float32)
    pick_dkeys = pick_dkeys + jnp.einsum(
        "kbs,ksf->kbf",
        owner_onehot,
        got_keys.reshape(kv_local, slot_count, KEY_BLOCK * HEAD_DIM),
        precision=lax.Precision.HIGHEST,
    ).reshape(kv_local, blocks_here, KEY_BLOCK, HEAD_DIM)
    pick_dvalues = pick_dvalues + jnp.einsum(
        "kbs,ksf->kbf",
        owner_onehot,
        got_values.reshape(kv_local, slot_count, KEY_BLOCK * HEAD_DIM),
        precision=lax.Precision.HIGHEST,
    ).reshape(kv_local, blocks_here, KEY_BLOCK, HEAD_DIM)
    key_total = (
        pick_dkeys.reshape(kv_local, tokens, HEAD_DIM)
        + jnp.repeat(pool_dkeys_here, POOL_BLOCK, axis=1) / POOL_BLOCK
    )
    value_total = (
        pick_dvalues.reshape(kv_local, tokens, HEAD_DIM)
        + jnp.repeat(pool_dvalues_here, POOL_BLOCK, axis=1) / POOL_BLOCK
    )
    grad_keys = (
        key_total.astype(jnp.bfloat16).transpose(1, 0, 2).reshape(tokens, kv_local * HEAD_DIM)
    )
    grad_values = (
        value_total.astype(jnp.bfloat16).transpose(1, 0, 2).reshape(tokens, kv_local * HEAD_DIM)
    )
    grad_queries = (
        (pool_dquery + pick_dquery)
        .astype(jnp.bfloat16)
        .transpose(2, 0, 1, 3)
        .reshape(tokens, kv_local * group_size * HEAD_DIM)
    )
    whole_rows = lax.all_gather(hidden_rows, "tp", axis=0, tiled=True)
    grad_weight = lax.psum_scatter(
        lax.dot_general(
            whole_rows, grad_queries, (((0,), (0,)), ((), ())), preferred_element_type=jnp.float32
        ),
        "kv",
        scatter_dimension=0,
        tiled=True,
    )
    return (grad_queries, grad_keys, grad_values, grad_weight)


def solution(mesh):
    placed = (
        P(("kv", "tp"), None),
        P("kv", "tp"),
        P("kv", "tp"),
        P("kv", "tp"),
        P(None, "tp", "kv"),
        P(None, "tp", "kv"),
        P("tp", "kv", None),
        P("kv", "tp"),
    )
    return jax.shard_map(
        body,
        mesh=mesh,
        in_specs=placed,
        out_specs=(P("kv", "tp"), P("kv", "tp"), P("kv", "tp"), P("kv", "tp")),
        check_vma=False,
    )
```

profile of v0, /device:TPU:0, one launch (start us, length us, event | category | flops | bytes accessed | tf_op | source)
XLA Modules:
  0.0 764.7 jit_solution(14092257159528464983)
XLA Ops:
  8.1 0.7 all-gather.2.cloned.1.call-update
  8.8 0.8 broadcast_in_dim_reshape.8
  9.5 0.8 broadcast_in_dim_reshape.9
  11.9 11.4 %scatter_fusion = s32[2,128]{1,0:T(2,128)S(1)} fusion(s32[2,128]{1,0:T(2,128)S(1)} %broadcast.386, s32[256]{0:T(256)S(1)} %get-tuple-element.29, s32[256]{0:T(256)S(1)} %get-tuple-element.31), kind=kCustom, calls=%fused_computation.4 | custom fusion | bytes 5120 | tf_op jit(solution)/shard_map/scatter | solution.py:129
  24.1 7.3 all-to-all-start
  31.4 6.5 all-to-all-done
  38.0 2.5 gather_fusion
  40.5 3.6 copy.98
  44.2 4.5 all-to-all-start.1
  48.8 4.4 reshape.402
  53.3 4.2 copy.90
  57.5 0.6 fusion.49
  58.1 0.6 sub.58
  58.9 57.0 %all_gather.9 = bf16[2,256,128]{2,1,0:T(8,128)(2,1)S(1)} all-gather(bf16[2,32,128]{2,1,0:T(8,128)(2,1)S(1)} %multiply_convert_fusion.5), channel_id=1, replica_groups=mesh['kv'=8,'tp'=4] {'kv'}, dimensions={1}, use_global_device_ids=true | all-gather | bytes 147456 | tf_op jit(solution)/shard_map/all_gather | solution.py:80
  115.9 32.5 %all_gather.10 = bf16[2,256,128]{2,1,0:T(8,128)(2,1)} all-gather(bf16[2,32,128]{2,1,0:T(8,128)(2,1)S(1)} %multiply_convert_fusion.4), channel_id=1, replica_groups=mesh['kv'=8,'tp'=4] {'kv'}, dimensions={1}, use_global_device_ids=true | all-gather | bytes 147456 | tf_op jit(solution)/shard_map/all_gather | solution.py:81
  148.7 5.3 multiply_convert_fusion.3
  154.0 4.5 fusion.8
  158.5 2.5 gather_fusion.2
  161.0 3.8 copy.103
  164.8 4.4 all-to-all-start.2
  169.5 5.8 multiply_reduce_fusion.1
  175.3 5.3 multiply_convert_fusion.1
  180.6 1.9 copy-done.8
  182.6 2.2 fusion.16
  184.8 6.2 fusion.19
  192.2 2.2 copy.148
  194.4 1.9 copy.102
  196.4 2.5 broadcast_compare_fusion
  198.9 3.6 pad_maximum_fusion
  202.5 4.2 gather_fusion.1
  206.9 3.6 pad_maximum_fusion.1
  210.5 4.3 gather_fusion.3
  214.8 9.8 %fusion.51 = f32[16,512,4,128]{3,1,2,0:T(8,128)} fusion(bf16[16,512,128,1]{2,1,3,0:T(8,128)(2,1)} %bitcast.210, bf16[16,4,128,128]{3,2,1,0:T(8,128)(2,1)S(1)} %bitcast.208), kind=kOutput, calls=%fused_computation.115 | convolution fusion | flops 1073741824 | bytes 20971520 | tf_op jit(solution)/shard_map/bgrd,bmd->bgrm/dot_general | solution.py:18
  224.6 8.2 %multiply_reduce_fusion = f32[16,4,128]{2,1,0:T(4,128)S(1)} fusion(bf16[16,4,128,128]{2,3,1,0:T(8,128)(2,1)S(1)} %bitcast.235, bf16[16,512,128,1]{2,1,3,0:T(8,128)(2,1)S(1)} %bitcast.238, f32[16,512,4,128]{3,1,2,0:T(8,128)} %fusion.51, f32[16,4,128]{2,1,0:T(4,128)S(1)} %bitcast.242, pred[16,128,512]{1,2,0:T(8,128)(4,1)S(1)} %copy-done.15), kind=kOutput, calls=%fused_computation.22 | convolution fusion | flops 1093656576 | bytes 22085632 | tf_op jit(solution)/shard_map/bgrm,bmd->bgrd/dot_general | solution.py:23
  232.8 21.0 %multiply_convert_fusion = bf16[16,4,128,512]{2,3,1,0:T(8,128)(2,1)S(1)} fusion(f32[16,512,4,128]{3,1,2,0:T(8,128)} %fusion.51, bf16[16,512,128,1]{2,1,3,0:T(8,128)(2,1)} %bitcast.237, bf16[16,4,128,128]{2,3,1,0:T(8,128)(2,1)} %bitcast.234, f32[16,4,128]{2,1,0:T(4,128)S(1)} %multiply_reduce_fusion, f32[16,4,128]{2,1,0:T(4,128)S(1)} %bitcast.243, ...), kind=kOutput, calls=%fused_computation.10 | convolution fusion | flops 1098907648 | bytes 30474240 | tf_op jit(solution)/shard_map/bgrd,bmd->bgrm/dot_general | solution.py:27
  253.9 4.6 convolution_multiply_fusion
  258.5 5.3 copy.110
  263.8 4.9 reshape.413
  268.7 6.3 add_convert_fusion
  275.0 16.0 %convolution_bitcast_fusion = f32[4096,1024]{0,1:T(8,128)} fusion(bf16[1024,1024]{0,1:T(8,128)(2,1)} %bitcast.225, bf16[1024,4096]{1,0:T(8,128)(2,1)} %all-gather.2.cloned.1.call-done), kind=kOutput, calls=%fused_computation.12 | convolution fusion | flops 8589934592 | bytes 27262976 | tf_op jit(solution)/shard_map/dot_general | solution.py:230
  291.0 7.8 %bitcast_multiply_fusion = f32[16,512,128]{2,1,0:T(8,128)} fusion(bf16[16,4,128,512]{2,3,1,0:T(8,128)(2,1)} %copy-done.3, bf16[16,4,128,128]{3,2,1,0:T(8,128)(2,1)S(1)} %bitcast.209), kind=kOutput, calls=%fused_computation.20 | convolution fusion | flops 1074790400 | bytes 14680064 | tf_op jit(solution)/shard_map/bgrm,bgrd->bmd/dot_general | solution.py:36
  298.9 2.5 broadcast.393.clone.1
  301.4 36.2 %scatter_fusion.1 = f32[2,128,32,128]{3,2,1,0:T(8,128)} fusion(f32[2,128,32,128]{3,2,1,0:T(8,128)} %broadcast.393.clone.1, s32[256]{0:T(256)S(1)} %get-tuple-element.29, f32[256,32,128]{2,1,0:T(8,128)} %bitcast.206), kind=kCustom, calls=%fused_computation.5 | custom fusion | bytes 12584960 | tf_op jit(solution)/shard_map/scatter | solution.py:182
  337.6 4.8 copy.112
  342.4 5.9 all-to-all-start.3
  348.2 11.1 %fusion.44 = f32[16,512,128,1]{2,1,3,0:T(8,128)} fusion(bf16[16,4,128,128]{2,3,1,0:T(8,128)(2,1)S(1)} %bitcast.236, f32[16,512,4,128]{3,1,2,0:T(8,128)} %fusion.51, f32[16,4,128]{2,1,0:T(4,128)S(1)} %bitcast.244, pred[16,128,512]{1,2,0:T(8,128)(4,1)} %broadcast_compare_fusion), kind=kOutput, calls=%fused_computation.110 | convolution fusion | flops 1090519040 | bytes 24150016 | tf_op jit(solution)/shard_map/bgrm,bgrd->bmd/dot_general | solution.py:39
  359.4 2.5 broadcast.393.clone
  361.9 36.3 %scatter_fusion.3 = f32[2,128,32,128]{3,2,1,0:T(8,128)} fusion(f32[2,128,32,128]{3,2,1,0:T(8,128)} %broadcast.393.clone, s32[256]{0:T(256)S(1)} %get-tuple-element.29, f32[256,32,128]{2,1,0:T(8,128)} %bitcast.216), kind=kCustom, calls=%fused_computation.7 | custom fusion | bytes 12584960 | tf_op jit(solution)/shard_map/scatter | solution.py:187
  398.2 4.9 copy.116
  403.1 130.6 %all-to-all-done.3 = f32[2,128,32,128]{3,2,0,1:T(8,128)} async-done(((f32[2,128,32,128]{3,2,0,1:T(8,128)}), f32[2,128,32,128]{3,2,0,1:T(8,128)}, u32[]{:S(2)}, u32[]{:S(2)}) %all-to-all-start.3) | async-done | bytes 4194336 | tf_op jit(solution)/shard_map/all_to_all | solution.py:190
  533.6 4.8 all-to-all-start.4
  538.5 0.7 convert_multiply_fusion.1
  539.2 0.7 convert_multiply_fusion
  539.9 2.6 copy.120
  542.5 5.8 reshape.493
  548.3 5.9 fusion.4
  554.6 24.3 %scatter_fusion.2 = f32[2,32,32,128]{3,2,1,0:T(8,128)S(1)} fusion(f32[2,32,32,128]{3,2,1,0:T(8,128)S(1)} %bitcast_add_fusion.1, s32[256]{0:T(256)S(1)} %copy-done.2, f32[256,32,128]{2,1,0:T(8,128)} %bitcast.207), kind=kCustom, calls=%fused_computation.6 | custom fusion | flops 1048576 | bytes 12584960 | tf_op jit(solution)/shard_map/scatter-add | solution.py:172
  579.5 62.0 %all-to-all-done.4 = f32[2,128,32,128]{3,2,0,1:T(8,128)} async-done(((f32[2,128,32,128]{3,2,0,1:T(8,128)}), f32[2,128,32,128]{3,2,0,1:T(8,128)}, u32[]{:S(2)}, u32[]{:S(2)}) %all-to-all-start.4) | async-done | bytes 4194336 | tf_op jit(solution)/shard_map/all_to_all | solution.py:191
  641.5 5.8 reshape.494
  647.3 5.9 fusion.2
  653.6 24.3 %scatter_fusion.4 = f32[2,32,32,128]{3,2,1,0:T(8,128)S(1)} fusion(f32[2,32,32,128]{3,2,1,0:T(8,128)S(1)} %bitcast_add_fusion, s32[256]{0:T(256)S(1)} %copy-done.2, f32[256,32,128]{2,1,0:T(8,128)} %bitcast.217), kind=kCustom, calls=%fused_computation.8 | custom fusion | flops 1048576 | bytes 12584960 | tf_op jit(solution)/shard_map/scatter-add | solution.py:177
  678.6 1.2 copy_bitcast_fusion
  679.8 74.1 %reduce-scatter.8.cloned.1.call-done = f32[512,1024]{0,1:T(8,128)} async-done(((f32[4096,1024]{0,1:T(8,128)}), f32[512,1024]{0,1:T(8,128)}) %reduce-scatter.8.cloned.1.call-update) | async-done | bytes 2097168 | tf_op jit(solution)/shard_map/reduce_scatter | solution.py:229
  753.9 2.9 copy.121
  (99 shorter events, 6.8 us)
Async XLA Ops:
  8.0 23.4 %copy-start = (bf16[1024,256]{1,0:T(8,128)(2,1)S(1)}, bf16[1024,256]{1,0:T(8,128)(2,1)}, u32[]{:S(2)}) copy-start(bf16[1024,256]{1,0:T(8,128)(2,1)} %param.10) | copy-start | bytes 1572868
  8.0 267.0 %all-gather.2.cloned.1.call-start = ((), (), s32[]{:S(2)}) async-start(), calls=%async_computation.10 | async-start | bytes 10485760 | tf_op jit(solution)/shard_map/all_gather | solution.py:228
  24.1 13.8 %all-to-all-start = ((s32[2,8,16]{2,0,1:T(2,128)}), s32[2,8,16]{2,0,1:T(2,128)S(1)}, u32[]{:S(2)}, u32[]{:S(2)}) async-start(s32[2,8,16]{2,0,1:T(2,128)} %copy.96), calls=%async_computation | async-start | bytes 16384 | tf_op jit(solution)/shard_map/all_to_all | solution.py:131
  44.2 9.1 %copy-start.18 = (f32[2,8,1024]{2,1,0:T(8,128)S(1)}, f32[2,8,1024]{2,1,0:T(8,128)}, u32[]{:S(2)}) copy-start(f32[2,8,1024]{2,1,0:T(8,128)} %param.12) | copy-start | bytes 196612
  44.2 120.7 %all-to-all-start.1 = ((bf16[2,128,32,128]{3,2,0,1:T(8,128)(2,1)}), bf16[2,128,32,128]{3,2,0,1:T(8,128)(2,1)}, u32[]{:S(2)}, u32[]{:S(2)}) async-start(bf16[2,128,32,128]{3,2,0,1:T(8,128)(2,1)} %copy.98), calls=%async_computation.1 | async-start | bytes 4194304 | tf_op jit(solution)/shard_map/all_to_all | solution.py:135
  53.2 4.3 copy-start.19
  53.2 5.6 copy-start.12
  148.7 5.3 copy-start.5
  161.0 8.4 %copy-start.13 = (bf16[2,4,1024,128]{2,3,1,0:T(8,128)(2,1)S(1)}, bf16[2,4,1024,128]{2,3,1,0:T(8,128)(2,1)}, u32[]{:S(2)}) copy-start(bf16[2,4,1024,128]{2,3,1,0:T(8,128)(2,1)} %get-tuple-element.22) | copy-start | bytes 6291460
  164.8 42.1 %all-to-all-start.2 = ((bf16[2,128,32,128]{3,2,0,1:T(8,128)(2,1)}), bf16[2,128,32,128]{3,2,0,1:T(8,128)(2,1)}, u32[]{:S(2)}, u32[]{:S(2)}) async-start(bf16[2,128,32,128]{3,2,0,1:T(8,128)(2,1)} %copy.103), calls=%async_computation.2 | async-start | bytes 4194304 | tf_op jit(solution)/shard_map/all_to_all | solution.py:138
  169.2 369.3 %reduce-scatter.4.cloned.1.call-start = ((), (), s32[]{:S(2)}) async-start(), calls=%async_computation.8 | async-start | bytes 147456 | tf_op jit(solution)/shard_map/reduce_scatter | solution.py:95
  169.5 5.8 copy-start.14
  169.5 5.8 copy-start.16
  169.5 5.8 copy-start.20
  175.3 7.3 copy-start.6
  180.6 2.0 copy-start.8
  184.8 354.4 %reduce-scatter.6.cloned.1.call-start = ((), (), s32[]{:S(2)}) async-start(), calls=%async_computation.9 | async-start | bytes 147456 | tf_op jit(solution)/shard_map/reduce_scatter | solution.py:98
  191.1 0.8 copy-start.21
  191.1 562.8 %reduce-scatter.8.cloned.1.call-start = ((), (), s32[]{:S(2)}) async-start(), calls=%async_computation.11 | async-start | bytes 18874368 | tf_op jit(solution)/shard_map/reduce_scatter | solution.py:229
  192.2 4.2 copy-start.17
  214.8 9.8 %copy-start.9 = (bf16[2,8,4,128,128]{3,4,2,1,0:T(8,128)(2,1)S(1)}, bf16[2,8,4,128,128]{3,4,2,1,0:T(8,128)(2,1)}, u32[]{:S(2)}) copy-start(bf16[2,8,4,128,128]{3,4,2,1,0:T(8,128)(2,1)} %copy.102) | copy-start | bytes 6291460
  214.8 9.8 %copy-start.11 = (bf16[256,32,128]{2,1,0:T(8,128)(2,1)S(1)}, bf16[256,32,128]{2,1,0:T(8,128)(2,1)}, u32[]{:S(2)}) copy-start(bf16[256,32,128]{2,1,0:T(8,128)(2,1)} %gather_fusion.3) | copy-start | bytes 6291460
  214.8 9.8 %copy-start.15 = (pred[16,128,512]{1,2,0:T(8,128)(4,1)S(1)}, pred[16,128,512]{1,2,0:T(8,128)(4,1)}, u32[]{:S(2)}) copy-start(pred[16,128,512]{1,2,0:T(8,128)(4,1)} %broadcast_compare_fusion) | copy-start | bytes 3145732
  232.8 21.0 %copy-start.4 = (bf16[256,32,128]{2,1,0:T(8,128)(2,1)S(1)}, bf16[256,32,128]{2,1,0:T(8,128)(2,1)}, u32[]{:S(2)}) copy-start(bf16[256,32,128]{2,1,0:T(8,128)(2,1)} %gather_fusion.1) | copy-start | bytes 6291460
  253.8 4.6 copy-start.3
  342.3 5.9 copy-start.10
  342.4 191.3 %all-to-all-start.3 = ((f32[2,128,32,128]{3,2,0,1:T(8,128)}), f32[2,128,32,128]{3,2,0,1:T(8,128)}, u32[]{:S(2)}, u32[]{:S(2)}) async-start(f32[2,128,32,128]{3,2,0,1:T(8,128)} %copy.112), calls=%async_computation.3 | async-start | bytes 8388608 | tf_op jit(solution)/shard_map/all_to_all | solution.py:190
  403.0 136.9 %copy-start.7 = (bf16[2,4,1024,128]{2,3,1,0:T(8,128)(2,1)S(1)}, bf16[2,4,1024,128]{2,3,1,0:T(8,128)(2,1)}, u32[]{:S(2)}) copy-start(bf16[2,4,1024,128]{2,3,1,0:T(8,128)(2,1)} %add_convert_fusion) | copy-start | bytes 6291460
  533.6 107.9 %all-to-all-start.4 = ((f32[2,128,32,128]{3,2,0,1:T(8,128)}), f32[2,128,32,128]{3,2,0,1:T(8,128)}, u32[]{:S(2)}, u32[]{:S(2)}) async-start(f32[2,128,32,128]{3,2,0,1:T(8,128)} %copy.116), calls=%async_computation.5 | async-start | bytes 8388608 | tf_op jit(solution)/shard_map/all_to_all | solution.py:191
  548.3 6.2 copy-start.2
  653.6 103.1 %copy-start.1 = (bf16[1024,256]{1,0:T(8,128)(2,1)S(1)}, bf16[1024,256]{1,0:T(8,128)(2,1)}, u32[]{:S(2)}) copy-start(bf16[1024,256]{1,0:T(8,128)(2,1)} %param.10) | copy-start | bytes 1572868
Sparse Core Ops, SparseCore 0:
  10.4 60.9 all-gather.1
Sparse Core Ops, SparseCore 1:
  184.9 63.5 reduce-scatter.3
  252.2 61.3 reduce-scatter.5
  317.2 436.6 reduce-scatter.7
where the time goes:
time: 774 us; the launch traced here: 765 us
  waiting for transfers between devices  274 us (35%)
  local copies, waits for them, and re-layouts  169 us (22%)
  matrix products  121 us (16%)
  blocking collectives  89.5 us (12%)
  other arithmetic  67.7 us (9%)
  starting transfers between devices  27.5 us (4%)
  between operations  16.5 us (2%)
    all_to_all x1, waiting for transfers between devices, body(): lax.all_to_all(back_keys, 'kv', split_axis=1, concat_axis=1, tiled=True)  131 us
    reduce_scatter x1, waiting for transfers between devices, body(): lax.psum_scatter(lax.dot_general(whole_rows, grad_queries, (((0,), (0,)),...  74.1 us
    all_to_all x1, waiting for transfers between devices, body(): lax.all_to_all(back_values, 'kv', split_axis=1, concat_axis=1, tiled=True)  62 us
    all_gather x1, blocking collectives, body(): lax.all_gather(pooled_keys, 'kv', axis=1, tiled=True)  57 us
    scatter x2, local copies, waits for them, and re-layouts, body(): back_values = jnp.zeros((kv_local, slot_count, KEY_BLOCK, HEAD_DIM), jnp....  41.2 us
    scatter x2, local copies, waits for them, and re-layouts, body(): back_keys = jnp.zeros((kv_local, slot_count, KEY_BLOCK, HEAD_DIM), jnp.fl...  41 us
    all_gather x1, blocking collectives, body(): lax.all_gather(pooled_values, 'kv', axis=1, tiled=True)  32.5 us
    dot_general x2, matrix products, attend_back(): jnp.einsum('bgrd,bmd->bgrm', cotangent, value_set, preferred_element_type...  26.3 us
  transfers between devices with their start and end apart: 9, of which 5 were waited for; matrix products, arithmetic and copies ran while one was open for 46% of the time, Pallas kernels for 0%

commit v1 on v0

v1 whole, which is shorter than its diff:
```python
import functools

import jax
import jax.numpy as jnp
from jax import lax
from jax.experimental import pallas as pl
from jax.experimental.pallas import tpu as pltpu
from jax.sharding import PartitionSpec as P

HEADS = 32
KV_HEADS = 8
HEAD_DIM = 128
QUERY_BLOCK = 128
KEY_BLOCK = 32
POOL_BLOCK = 32
CHOSEN = 16
CAP = 16

F32 = jnp.float32
BF16 = jnp.bfloat16


def dot_nt(a, b):
    return lax.dot_general(a, b, (((1,), (1,)), ((), ())), preferred_element_type=F32)


def dot_nn(a, b):
    return lax.dot_general(a, b, (((1,), (0,)), ((), ())), preferred_element_type=F32)


def branch_back(keys, values, query_stack, cot_stack, log_row, mask, scale):
    scores = dot_nt(keys, query_stack) * scale
    weights = jnp.where(mask, jnp.exp(scores - log_row), 0.0)
    weights_low = weights.astype(BF16)
    grad_prob = dot_nt(values, cot_stack)
    delta = jnp.sum(weights_low.astype(F32) * grad_prob, axis=0, keepdims=True)
    dscore = (weights * (grad_prob - delta)).astype(BF16)
    dquery = dot_nn(keys.T, dscore)
    return dquery, dot_nn(dscore, query_stack) * scale, dot_nn(weights_low, cot_stack)


def attend_kernel(
    group, section, kv_count, scale,
    place_ref, lists_ref, slot_ref, own_ref,
    q_ref, g_ref, gate_ref, log_ref, k_ref, v_ref,
    dq_ref, send_ref, kept_ref,
    pooled_k, pooled_v, pool_dk, pool_dv, kept,
):
    head = pl.program_id(0)
    step = pl.program_id(1)
    pool_count = pooled_k.shape[0]
    tokens = kept_ref.shape[0]
    pool_here = pool_count // kv_count
    chunk = 8 * POOL_BLOCK

    @pl.when(step == 0)
    def _():
        send_ref[...] = jnp.zeros_like(send_ref)
        kept[...] = jnp.zeros_like(kept)
        pool_dk[...] = jnp.zeros_like(pool_dk)
        pool_dv[...] = jnp.zeros_like(pool_dv)
        pick = (
            lax.broadcasted_iota(jnp.int32, (16, 2 * chunk), 1) // POOL_BLOCK
            == lax.broadcasted_iota(jnp.int32, (16, 2 * chunk), 0)
        ).astype(BF16)

        def pool(i, carry):
            rows = pl.ds(pl.multiple_of(i * 2 * chunk, 2 * chunk), 2 * chunk)
            dest = pl.ds(pl.multiple_of(i * 16, 16), 16)
            pooled_k[dest, :] = (dot_nn(pick, k_ref[rows, :]) / POOL_BLOCK).astype(BF16)
            pooled_v[dest, :] = (dot_nn(pick, v_ref[rows, :]) / POOL_BLOCK).astype(BF16)
            return carry

        lax.fori_loop(0, pool_count // 16, pool, 0)

    query_stack = jnp.concatenate(
        [q_ref[:, r * HEAD_DIM : (r + 1) * HEAD_DIM] for r in range(group)], axis=0
    )
    gates = gate_ref[0].T
    grads = [g_ref[:, r * HEAD_DIM : (r + 1) * HEAD_DIM].astype(F32) for r in range(group)]

    def gated(branch):
        cols = [gates[:, branch * group + r : branch * group + r + 1] for r in range(group)]
        return jnp.concatenate([(c * g).astype(BF16) for c, g in zip(cols, grads)], axis=0)

    def log_row(branch):
        return jnp.concatenate(
            [log_ref[0, branch * group + r : branch * group + r + 1, :] for r in range(group)],
            axis=1,
        )

    width = group * QUERY_BLOCK
    first = place_ref[0] * tokens + step * QUERY_BLOCK
    query_pos = first + lax.broadcasted_iota(jnp.int32, (1, width), 1) % QUERY_BLOCK

    pool_end = (
        lax.broadcasted_iota(jnp.int32, (pool_count, width), 0) * POOL_BLOCK + POOL_BLOCK - 1
    )
    dq_pool, dk, dv = branch_back(
        pooled_k[...], pooled_v[...], query_stack, gated(0), log_row(0),
        pool_end <= query_pos, scale,
    )
    pool_dk[...] += dk
    pool_dv[...] += dv

    ids = [lists_ref[head, step * CHOSEN + c] for c in range(CHOSEN)]
    rows = [pl.ds(pl.multiple_of(i * KEY_BLOCK, KEY_BLOCK), KEY_BLOCK) for i in ids]
    keys = jnp.concatenate([k_ref[r, :] for r in rows], axis=0)
    values = jnp.concatenate([v_ref[r, :] for r in rows], axis=0)
    offset = lax.broadcasted_iota(jnp.int32, (KEY_BLOCK, width), 0)
    key_pos = jnp.concatenate([offset + i * KEY_BLOCK for i in ids], axis=0)
    dq_pick, dk, dv = branch_back(
        keys, values, query_stack, gated(1), log_row(1), key_pos <= query_pos, scale
    )
    both = jnp.concatenate([dk, dv], axis=1)
    for c in range(CHOSEN):
        part = both[c * KEY_BLOCK : (c + 1) * KEY_BLOCK]
        slot = pl.multiple_of(slot_ref[head, step * CHOSEN + c], KEY_BLOCK)
        own = pl.multiple_of(own_ref[head, step * CHOSEN + c], KEY_BLOCK)
        send_ref[pl.ds(slot, KEY_BLOCK), :] = part.astype(BF16)
        kept[pl.ds(own, KEY_BLOCK), :] += part

    dq = (dq_pool + dq_pick) * scale
    for r in range(group):
        dq_ref[:, r * HEAD_DIM : (r + 1) * HEAD_DIM] = dq[
            :, r * QUERY_BLOCK : (r + 1) * QUERY_BLOCK
        ].T.astype(BF16)

    @pl.when(step == pl.num_programs(1) - 1)
    def _():
        kept_ref[...] = kept[:tokens, :]
        for owner in range(kv_count):
            at = owner * section + CAP * KEY_BLOCK
            here = slice(owner * pool_here, (owner + 1) * pool_here)
            send_ref[at : at + pool_here, :HEAD_DIM] = pool_dk[here, :].astype(BF16)
            send_ref[at : at + pool_here, HEAD_DIM:] = pool_dv[here, :].astype(BF16)


def settle_kernel(section, kv_count, place_ref, asked_ref, got_ref, kept_ref, gk_ref, gv_ref, acc):
    head = pl.program_id(0)
    tokens = kept_ref.shape[0]
    pool_here = tokens // POOL_BLOCK
    at = CAP * KEY_BLOCK
    pooled = sum(
        got_ref[i * section + at : i * section + at + pool_here, :].astype(F32)
        for i in range(kv_count)
    ) / POOL_BLOCK
    for j in range(pool_here):
        rows = slice(j * POOL_BLOCK, (j + 1) * POOL_BLOCK)
        acc[rows, :] = kept_ref[rows, :] + pooled[j : j + 1, :]

    def source(i, carry):
        other = lax.rem(place_ref[0] + 1 + i, kv_count)
        for c in range(CAP):
            block = asked_ref[head, other * CAP + c]
            rows = pl.ds(pl.multiple_of(block * KEY_BLOCK, KEY_BLOCK), KEY_BLOCK)
            came = pl.ds(pl.multiple_of(other * section + c * KEY_BLOCK, KEY_BLOCK), KEY_BLOCK)
            acc[rows, :] += got_ref[came, :].astype(F32)
        return carry

    lax.fori_loop(0, kv_count - 1, source, 0)
    gk_ref[...] = acc[:, :HEAD_DIM].astype(BF16)
    gv_ref[...] = acc[:, HEAD_DIM:].astype(BF16)


def body(hidden_rows, queries, key_rows, value_rows, branch_gates, log_sums, chosen, out_grad):
    kv_count = lax.axis_size("kv")
    kv_index = lax.axis_index("kv")
    tokens = queries.shape[0]
    kv_local = key_rows.shape[1] // HEAD_DIM
    group = HEADS // KV_HEADS
    scale = HEAD_DIM ** (-0.5)
    seq_len = tokens * kv_count
    steps = tokens // QUERY_BLOCK
    blocks_here = tokens // KEY_BLOCK
    pool_count = seq_len // POOL_BLOCK
    pool_here = tokens // POOL_BLOCK
    request_count = steps * CHOSEN
    section = CAP * KEY_BLOCK + pool_here
    slot_count = kv_count * CAP

    pair_rows = jnp.concatenate([key_rows, value_rows], axis=1)
    every_pair = lax.all_gather(pair_rows, "kv", axis=0, tiled=True)

    lists = chosen.reshape(kv_local, request_count)
    owners = lists // blocks_here
    local_block = lists % blocks_here
    remote = owners != kv_index
    order = jnp.arange(request_count, dtype=jnp.int32)
    rank_in = jnp.sum(
        (
            (owners[:, :, None] == owners[:, None, :]) & (order[None, None, :] < order[None, :, None])
        ).astype(jnp.int32),
        axis=-1,
    )
    slot_index = jnp.where(remote, owners * CAP + rank_in, slot_count)
    wanted = jnp.sum(
        jnp.where(
            slot_index[:, None, :] == jnp.arange(slot_count, dtype=jnp.int32)[None, :, None],
            local_block[:, None, :],
            0,
        ),
        axis=-1,
    )
    asked_for = lax.all_to_all(wanted, "kv", split_axis=1, concat_axis=1, tiled=True)
    slot_row = jnp.where(remote, owners * section + rank_in * KEY_BLOCK, kv_index * section)
    own_row = jnp.where(remote, tokens, local_block * KEY_BLOCK)
    place = kv_index.astype(jnp.int32).reshape(1)

    def per_head(array):
        return (
            array.reshape(2, kv_local, group, tokens)
            .transpose(1, 0, 2, 3)
            .reshape(kv_local, 2 * group, tokens)
        )

    pairs_flops = 2 * kv_local * group * tokens * HEAD_DIM * (pool_count + CHOSEN * KEY_BLOCK) * 5
    wide = 2 * HEAD_DIM
    grad_queries, send, kept = pl.pallas_call(
        functools.partial(attend_kernel, group, section, kv_count, scale),
        grid_spec=pltpu.PrefetchScalarGridSpec(
            num_scalar_prefetch=4,
            grid=(kv_local, steps),
            in_specs=[
                pl.BlockSpec((QUERY_BLOCK, group * HEAD_DIM), lambda h, b, *_: (b, h)),
                pl.BlockSpec((QUERY_BLOCK, group * HEAD_DIM), lambda h, b, *_: (b, h)),
                pl.BlockSpec((1, 2 * group, QUERY_BLOCK), lambda h, b, *_: (h, 0, b)),
                pl.BlockSpec((1, 2 * group, QUERY_BLOCK), lambda h, b, *_: (h, 0, b)),
                pl.BlockSpec((seq_len, HEAD_DIM), lambda h, b, *_: (0, h)),
                pl.BlockSpec((seq_len, HEAD_DIM), lambda h, b, *_: (0, kv_local + h)),
            ],
            out_specs=[
                pl.BlockSpec((QUERY_BLOCK, group * HEAD_DIM), lambda h, b, *_: (b, h)),
                pl.BlockSpec((kv_count * section, wide), lambda h, b, *_: (0, h)),
                pl.BlockSpec((tokens, wide), lambda h, b, *_: (0, h)),
            ],
            scratch_shapes=[
                pltpu.VMEM((pool_count, HEAD_DIM), BF16),
                pltpu.VMEM((pool_count, HEAD_DIM), BF16),
                pltpu.VMEM((pool_count, HEAD_DIM), F32),
                pltpu.VMEM((pool_count, HEAD_DIM), F32),
                pltpu.VMEM((tokens + KEY_BLOCK, wide), F32),
            ],
        ),
        out_shape=[
            jax.ShapeDtypeStruct((tokens, kv_local * group * HEAD_DIM), BF16),
            jax.ShapeDtypeStruct((kv_count * section, kv_local * wide), BF16),
            jax.ShapeDtypeStruct((tokens, kv_local * wide), F32),
        ],
        cost_estimate=pl.CostEstimate(
            flops=pairs_flops, bytes_accessed=24 * 2**20, transcendentals=0
        ),
        name="attend_back",
    )(
        place, lists, slot_row, own_row,
        queries, out_grad, per_head(branch_gates), per_head(log_sums), every_pair, every_pair,
    )

    got = lax.all_to_all(send, "kv", split_axis=0, concat_axis=0, tiled=True)

    hidden_late, _ = lax.optimization_barrier((hidden_rows, every_pair))
    whole_rows = lax.all_gather(hidden_late, "tp", axis=0, tiled=True)
    terms = lax.dot_general(
        whole_rows, grad_queries, (((0,), (0,)), ((), ())), preferred_element_type=F32
    ).astype(BF16)
    grad_weight = lax.psum_scatter(terms, "kv", scatter_dimension=0, tiled=True).astype(F32)

    grad_keys, grad_values = pl.pallas_call(
        functools.partial(settle_kernel, section, kv_count),
        grid_spec=pltpu.PrefetchScalarGridSpec(
            num_scalar_prefetch=2,
            grid=(kv_local,),
            in_specs=[
                pl.BlockSpec((kv_count * section, wide), lambda h, *_: (0, h)),
                pl.BlockSpec((tokens, wide), lambda h, *_: (0, h)),
            ],
            out_specs=[
                pl.BlockSpec((tokens, HEAD_DIM), lambda h, *_: (0, h)),
                pl.BlockSpec((tokens, HEAD_DIM), lambda h, *_: (0, h)),
            ],
            scratch_shapes=[pltpu.VMEM((tokens, wide), F32)],
        ),
        out_shape=[
            jax.ShapeDtypeStruct((tokens, kv_local * HEAD_DIM), BF16),
            jax.ShapeDtypeStruct((tokens, kv_local * HEAD_DIM), BF16),
        ],
        cost_estimate=pl.CostEstimate(
            flops=4 * 2**20, bytes_accessed=8 * 2**20, transcendentals=0
        ),
        name="settle",
    )(place, asked_for, got, kept)
    return (grad_queries, grad_keys, grad_values, grad_weight)


def solution(mesh):
    placed = (
        P(("kv", "tp"), None),
        P("kv", "tp"),
        P("kv", "tp"),
        P("kv", "tp"),
        P(None, "tp", "kv"),
        P(None, "tp", "kv"),
        P("tp", "kv", None),
        P("kv", "tp"),
    )
    return jax.shard_map(
        body,
        mesh=mesh,
        in_specs=placed,
        out_specs=(P("kv", "tp"), P("kv", "tp"), P("kv", "tp"), P("kv", "tp")),
        check_vma=False,
    )
```

time: 774 us -> 452 us (0.58); the launches traced: 765 us -> 452 us
  local copies, waits for them, and re-layouts: 169 us -> 2.21 us
  matrix products: 121 us -> 14.9 us
  blocking collectives: 89.5 us -> 11.9 us
  waiting for transfers between devices: 274 us -> 349 us
  other arithmetic: 67.7 us -> 6.46 us
  Pallas kernels: 0 us -> 48.8 us
  starting transfers between devices: 27.5 us -> 4.7 us
    all_gather x1 -> x2, waiting for transfers between devices: 0.01 us -> 140 us  [the longest x1 128 us: body(): every_pair = lax.all_gather(pair_rows, 'kv', axis=0, tiled=True)]
    dot_general x14 -> x0, matrix products: 105 us -> none  [the longest x2 26.3 us: attend_back(): jnp.einsum('bgrd,bmd->bgrm', cotangent, value_set, preferred_element_type...]
    scatter x5 -> x0, local copies, waits for them, and re-layouts: 93.6 us -> none  [the longest x2 41.2 us: body(): back_values = jnp.zeros((kv_local, slot_count, KEY_BLOCK, HEAD_DIM), jnp....]
    all_gather x2 -> x0, blocking collectives: 89.5 us -> none  [the longest x1 57 us: body(): lax.all_gather(pooled_keys, 'kv', axis=1, tiled=True)]
    pallas_call x0 -> x2, Pallas kernels: none -> 48.8 us  [the longest x1 43.6 us: body(): pl.pallas_call(functools.partial(attend_kernel, group, section, kv_count,...]
    scatter-add x2 -> x0, other arithmetic: 48.6 us -> none  [the longest x1 24.3 us: body(): pick_dkeys = jnp.zeros((kv_local, blocks_here, KEY_BLOCK, HEAD_DIM), jnp....]
    all_to_all x5 -> x1, waiting for transfers between devices: 199 us -> 156 us  [body(): got = lax.all_to_all(send, 'kv', split_axis=0, concat_axis=0, tiled=True)]
    reshape x9 -> x7, local copies, waits for them, and re-layouts: 27.7 us -> 1.45 us  [the longest x2 1.31 us: per_head(): return array.reshape(2, kv_local, group, tokens).transpose(1, 0, 2, 3).re...]
  transfers between devices with their start and end apart: 9 -> 4, of which waited for: 5 -> 4; matrix products, arithmetic and copies ran while one was open for 46% -> 1% of each run, Pallas kernels for 0% -> 11%
where the time goes in v1:
time: 452 us
  waiting for transfers between devices  349 us (77%)
  Pallas kernels  48.8 us (11%)
  matrix products  14.9 us (3%)
  between operations  13.8 us (3%)
  blocking collectives  11.9 us (3%)
  other arithmetic  6.46 us (1%)
  starting transfers between devices  4.7 us (1%)
    all_to_all x1, waiting for transfers between devices, body(): got = lax.all_to_all(send, 'kv', split_axis=0, concat_axis=0, tiled=True)  156 us
    all_gather x1, waiting for transfers between devices, body(): every_pair = lax.all_gather(pair_rows, 'kv', axis=0, tiled=True)  128 us
    reduce_scatter x1, waiting for transfers between devices, body(): lax.psum_scatter(terms, 'kv', scatter_dimension=0, tiled=True).astype(F32)  53.1 us
    pallas_call x1, Pallas kernels, body(): pl.pallas_call(functools.partial(attend_kernel, group, section, kv_count,...  43.6 us
    dot_general x1, matrix products, body(): lax.dot_general(whole_rows, grad_queries, (((0,), (0,)), ((), ())), prefe...  14.9 us
    all_to_all x1, blocking collectives, body(): lax.all_to_all(wanted, 'kv', split_axis=1, concat_axis=1, tiled=True)  11.9 us
    all_gather x1, waiting for transfers between devices, body(): whole_rows = lax.all_gather(hidden_late, 'tp', axis=0, tiled=True)  11.6 us
  transfers between devices with their start and end apart: 4, of which 4 were waited for; matrix products, arithmetic and copies ran while one was open for 1% of the time, Pallas kernels for 11%

profile of v1, /device:TPU:0, one launch (start us, length us, event | category | flops | bytes accessed | tf_op | source)
XLA Modules:
  0.0 451.8 jit_solution(16493698235967662099)
XLA Ops:
  7.2 0.0 all-gather.3.cloned.1.call-start
  7.2 2.2 pad_maximum_fusion
  9.5 0.0 copy-start.2
  9.5 0.0 copy-start
  9.5 0.0 copy-start.1
  9.5 0.0 all-gather.3.cloned.1.call-update
  9.5 0.0 all-gather.5.cloned.1.call-start
  9.5 128.4 %all-gather.3.cloned.1.call-done.k_ref.v_ref = bf16[8192,512]{1,0:T(8,128)(2,1)} async-done(((bf16[1024,512]{1,0:T(8,128)(2,1)}), bf16[8192,512]{1,0:T(8,128)(2,1)}) %all-gather.3.cloned.1.call-update) | async-done | bytes 8388624 | tf_op jit(solution)/shard_map/all_gather | solution.py:183
  137.9 0.0 all-gather.5.cloned.1.call-update
  137.9 0.0 reduce-scatter.2.cloned.1.call-start
  138.0 0.0 copy-done.2
  138.0 0.1 reshape.138.lists_ref
  138.1 0.0 copy-done
  138.1 0.0 copy-start.3
  138.1 0.7 reshape.140.gate_ref
  138.8 0.0 copy-done.1
  138.8 0.7 reshape.142.log_ref
  139.5 0.5 multiply_select_fusion
  140.0 0.2 convert_reduce_fusion
  140.2 0.6 add_select_fusion
  140.8 0.0 copy-done.3
  140.8 43.6 %attend_back.1 = (bf16[1024,1024]{1,0:T(8,128)(2,1)}, bf16[4352,512]{1,0:T(8,128)(2,1)}, f32[1024,512]{1,0:T(8,128)}) custom-call(s32[1]{0:T(128)} %bitcast.place_ref, s32[2,128]{1,0:T(2,128)} %copy-done.3, s32[2,128]{1,0:T(2,128)} %get-tuple-element.20.slot_ref, s32[2,128]{1,0:T(2,128)} %get-tuple-element.16.own_ref, bf16[1024,1024]{1,0:T(8,128)(2,1)} %q_ref.1, ...), custom_call_target="tpu_custom_call" | custom-call | flops 8053063680 | bytes 25165824 | tf_op jit(solution)/shard_map/attend_back/pallas_call | solution.py:219
  184.4 11.6 %all-gather.5.cloned.1.call-done = bf16[1024,4096]{1,0:T(8,128)(2,1)} async-done(((bf16[256,4096]{1,0:T(8,128)(2,1)}), bf16[1024,4096]{1,0:T(8,128)(2,1)}) %all-gather.5.cloned.1.call-update) | async-done | bytes 8388624 | tf_op jit(solution)/shard_map/all_gather | solution.py:262
  195.9 14.9 %convolution_convert_fusion = bf16[4096,1024]{1,0:T(8,128)(2,1)} fusion(bf16[1024,4096]{1,0:T(8,128)(2,1)} %all-gather.5.cloned.1.call-done, bf16[1024,1024]{1,0:T(8,128)(2,1)} %get-tuple-element.6), kind=kOutput, calls=%fused_computation | convolution fusion | flops 8594128896 | bytes 18874368 | tf_op jit(solution)/shard_map/dot_general | solution.py:263
  210.8 0.0 reduce-scatter.2.cloned.1.call-update
  210.9 0.1 select_reduce_fusion
  211.0 0.1 all_to_all.14
  211.1 11.9 %all_to_all.22 = s32[2,8,16]{2,0,1:T(2,128)S(1)} all-to-all(s32[2,8,16]{2,0,1:T(2,128)S(1)} %copy.23), channel_id=1, replica_groups=mesh['kv'=8,'tp'=4] {'kv'}, dimensions={1} | all-to-all | bytes 2048 | tf_op jit(solution)/shard_map/all_to_all | solution.py:205
  223.0 4.6 %all-to-all-start.1 = ((bf16[8,544,512]{2,1,0:T(8,128)(2,1)}), bf16[8,544,512]{2,1,0:T(8,128)(2,1)}, u32[]{:S(2)}, u32[]{:S(2)}) async-start(bf16[8,544,512]{2,1,0:T(8,128)(2,1)} %bitcast.11), calls=%async_computation.1 | async-start | bytes 8912896 | tf_op jit(solution)/shard_map/all_to_all | solution.py:259
  227.6 0.7 all_to_all.16.asked_ref
  228.2 155.9 %all-to-all-done.1 = bf16[8,544,512]{2,1,0:T(8,128)(2,1)} async-done(((bf16[8,544,512]{2,1,0:T(8,128)(2,1)}), bf16[8,544,512]{2,1,0:T(8,128)(2,1)}, u32[]{:S(2)}, u32[]{:S(2)}) %all-to-all-start.1) | async-done | bytes 4456480 | tf_op jit(solution)/shard_map/all_to_all | solution.py:259
  384.2 5.3 %settle.1 = (bf16[1024,256]{1,0:T(8,128)(2,1)}, bf16[1024,256]{1,0:T(8,128)(2,1)}) custom-call(s32[1]{0:T(128)} %bitcast.place_ref, s32[2,128]{1,0:T(2,128)} %all_to_all.16.asked_ref, bf16[4352,512]{1,0:T(8,128)(2,1)} %bitcast.4.got_ref, f32[1024,512]{1,0:T(8,128)} %get-tuple-element.12.kept_ref), custom_call_target="tpu_custom_call" | custom-call | flops 4194304 | bytes 8388608 | tf_op jit(solution)/shard_map/settle/pallas_call | solution.py:268
  389.4 53.1 %reduce-scatter.2.cloned.1.call-done = bf16[512,1024]{1,0:T(8,128)(2,1)} async-done(((bf16[4096,1024]{1,0:T(8,128)(2,1)}), bf16[512,1024]{1,0:T(8,128)(2,1)}) %reduce-scatter.2.cloned.1.call-update) | async-done | bytes 1048592 | tf_op jit(solution)/shard_map/reduce_scatter | solution.py:266
  442.5 2.8 convert_element_type.11
  (7 shorter events, 0.1 us)
Async XLA Ops:
  7.2 130.7 %all-gather.3.cloned.1.call-start = ((), (), s32[]{:S(2)}) async-start(), calls=%async_computation.3 | async-start | bytes 9437184 | tf_op jit(solution)/shard_map/all_gather | solution.py:183
  9.5 128.5 %copy-start.2 = (s32[2,8,16]{2,1,0:T(8,128)S(1)}, s32[2,8,16]{2,1,0:T(8,128)}, u32[]{:S(2)}) copy-start(s32[2,8,16]{2,1,0:T(8,128)} %param.14) | copy-start | bytes 3076
  9.5 128.6 %copy-start = (f32[2,8,1024]{2,1,0:T(8,128)S(1)}, f32[2,8,1024]{2,1,0:T(8,128)}, u32[]{:S(2)}) copy-start(f32[2,8,1024]{2,1,0:T(8,128)} %param.12) | copy-start | bytes 196612
  9.5 129.3 %copy-start.1 = (f32[2,8,1024]{2,1,0:T(8,128)S(1)}, f32[2,8,1024]{2,1,0:T(8,128)}, u32[]{:S(2)}) copy-start(f32[2,8,1024]{2,1,0:T(8,128)} %param.13) | copy-start | bytes 196612
  9.5 186.4 %all-gather.5.cloned.1.call-start = ((), (), s32[]{:S(2)}) async-start(), calls=%async_computation.4 | async-start | bytes 10485760 | tf_op jit(solution)/shard_map/all_gather | solution.py:262
  137.9 304.6 %reduce-scatter.2.cloned.1.call-start = ((), (), s32[]{:S(2)}) async-start(), calls=%async_computation.5 | async-start | bytes 9437184 | tf_op jit(solution)/shard_map/reduce_scatter | solution.py:266
  138.1 2.7 copy-start.3
  223.0 161.2 %all-to-all-start.1 = ((bf16[8,544,512]{2,1,0:T(8,128)(2,1)}), bf16[8,544,512]{2,1,0:T(8,128)(2,1)}, u32[]{:S(2)}, u32[]{:S(2)}) async-start(bf16[8,544,512]{2,1,0:T(8,128)(2,1)} %bitcast.11), calls=%async_computation.1 | async-start | bytes 8912896 | tf_op jit(solution)/shard_map/all_to_all | solution.py:259
Sparse Core Ops, SparseCore 0:
  10.7 127.1 all-gather.2
  139.5 56.4 all-gather.4
  211.0 231.4 reduce-scatter.1
